TPU v7x, 32 devices: a whole 2x2x4 slice. The times are simulated.
32 devices in a mesh: ep: 8 (over z, x), tp: 4 (over y, core).
Axes of the slice: x: 2, y: 2, z: 4, core: 2. Of those that a mesh axis runs over, the one named last changes fastest.
Arguments:
- mixer_input: bfloat16 [4096, 2048], P('ep', 'tp'), may hold values from -6 to 6
- mixer_gain: float32 [2048], replicated, may hold values from 0.1 to 1.9
- w_query: bfloat16 [2048, 1024], P(None, 'tp'), may hold values from -0.125 to 0.125
- w_key: bfloat16 [2048, 128], replicated, may hold values from -0.125 to 0.125
- w_value: bfloat16 [2048, 128], replicated, may hold values from -0.125 to 0.125
- query_gain: float32 [64], replicated, may hold values from 0.5 to 10
- key_gain: float32 [64], replicated, may hold values from 0.5 to 10
- sink_logit: float32 [16], P('tp'), may hold values from 1 to 5
- w_output: bfloat16 [1024, 2048], P('tp'), may hold values from -0.1875 to 0.1875
- expert_input: bfloat16 [1024, 2048], P('ep'), may hold values from -6 to 6
- expert_gain: float32 [2048], replicated, may hold values from 0.1 to 1.9
- route_ids: int32 [1024, 4], P('ep'), may hold values from 0 to 7, all different within a row; in each aligned block of 128 rows (0 to 127, 128 to 255, ...) at most 128 rows name the same one
- route_weight: float32 [1024, 4], P('ep'), may hold values from 0.2 to 1.2
- expert_gate: bfloat16 [8, 2048, 2048], P('ep', None, 'tp'), may hold values from -0.125 to 0.125
- expert_up: bfloat16 [8, 2048, 2048], P('ep', None, 'tp'), may hold values from -0.125 to 0.125
- expert_down: bfloat16 [8, 2048, 2048], P('ep', None, 'tp'), may hold values from -0.125 to 0.125
- shared_gate: bfloat16 [2048, 1024], P(None, 'tp'), may hold values from -0.125 to 0.125
- shared_up: bfloat16 [2048, 1024], P(None, 'tp'), may hold values from -0.125 to 0.125
- shared_down: bfloat16 [1024, 2048], P(None, 'tp'), may hold values from -0.1875 to 0.1875
Outputs:
- mixer_output: bfloat16 [4096, 2048], P('ep', 'tp')
- expert_output: bfloat16 [1024, 2048], P('ep', 'tp')
Inputs may be any that keep to these rules, and one draw needn't show every extreme that they name: `route_ids`: each row names 4 different experts. In the rows of one index of ep (aligned blocks of 128 rows) no expert is named by more than 128 rows, a bound that some block reaches.
All inputs are finite; a program needn't handle non-finite values.
Results may differ from a plain program's by a relative error of at most 0.018.
The roundings to bfloat16 on the way count: a program that leaves them out, or rounds other values in their place, can miss the bound.
Values may be sent and summed in bfloat16 or wider, within the bound.
A program may use at most 64 MiB of HBM per device.

v0:
```python
import jax
import jax.numpy as jnp
from jax import lax
from jax.sharding import PartitionSpec as P

D = 2048
HEAD = 64
KV_HEADS = 2
WINDOW = 128
TOPK = 4


EPSILON = 1e-06


def from_behind(value, axis, steps):
    count = lax.axis_size(axis)
    first, last = (max(0, -steps), min(count, count - steps))
    return lax.ppermute(value, axis, [(source, source + steps) for source in range(first, last)])


def head_norm(matrix, gain_vector):
    return (
        matrix
        * lax.rsqrt(jnp.mean(matrix * matrix, axis=-1, keepdims=True) + EPSILON)
        * gain_vector
    )


def band_attend(queries, keys_own, values_own, keys_prev, values_prev, sink_logit, first_row):
    row_count = queries.shape[0]
    head_count = queries.shape[1]
    blocks = row_count // WINDOW
    keys_all = jnp.concatenate([keys_prev, keys_own], axis=0)
    values_all = jnp.concatenate([values_prev, values_own], axis=0)
    key_band = jnp.concatenate(
        [
            keys_all[:row_count].reshape(blocks, WINDOW, HEAD),
            keys_own.reshape(blocks, WINDOW, HEAD),
        ],
        axis=1,
    )
    value_band = jnp.concatenate(
        [
            values_all[:row_count].reshape(blocks, WINDOW, HEAD),
            values_own.reshape(blocks, WINDOW, HEAD),
        ],
        axis=1,
    )
    query_blocks = queries.reshape(blocks, WINDOW, head_count, HEAD)
    scores = jnp.einsum(
        "nqhd,nkd->nhqk", query_blocks, key_band, preferred_element_type=jnp.float32
    ) * HEAD ** (-0.5)
    query_idx = jnp.arange(WINDOW, dtype=jnp.int32)[:, None]
    key_idx = jnp.arange(2 * WINDOW, dtype=jnp.int32)[None, :]
    relative = query_idx + WINDOW - key_idx
    block_idx = jnp.arange(blocks, dtype=jnp.int32)[:, None, None]
    key_pos = first_row + block_idx * WINDOW - WINDOW + key_idx[None]
    allowed = ((relative >= 0) & (relative < WINDOW))[None] & (key_pos >= 0)
    allowed = allowed[:, None]
    masked = jnp.where(allowed, scores, -jnp.inf)
    sink_column = sink_logit.reshape(1, head_count, 1, 1)
    peak_score = jnp.maximum(jnp.max(masked, axis=-1, keepdims=True), sink_column)
    exponent = jnp.exp(masked - peak_score)
    denominator = jnp.sum(exponent, axis=-1, keepdims=True) + jnp.exp(sink_column - peak_score)
    probability = (exponent / denominator).astype(jnp.bfloat16)
    mixed_rows = jnp.einsum(
        "nhqk,nkd->nqhd", probability, value_band, preferred_element_type=jnp.float32
    )
    return mixed_rows.reshape(row_count, head_count * HEAD).astype(jnp.bfloat16)


def shards(
    mixer_input,
    mixer_gain,
    w_query,
    w_key,
    w_value,
    query_gain,
    key_gain,
    sink_logit,
    w_output,
    expert_input,
    expert_gain,
    route_ids,
    route_weight,
    expert_gate,
    expert_up,
    expert_down,
    shared_gate,
    shared_up,
    shared_down,
):
    tp_count = lax.axis_size("tp")
    ep_count = lax.axis_size("ep")
    rows_local = mixer_input.shape[0]
    heads_local = w_query.shape[1] // HEAD
    kv_index = lax.axis_index("tp") // (tp_count // KV_HEADS)
    key_cols = lax.dynamic_slice_in_dim(w_key, kv_index * HEAD, HEAD, 1)
    value_cols = lax.dynamic_slice_in_dim(w_value, kv_index * HEAD, HEAD, 1)
    portion_float = lax.all_gather(mixer_input, "tp", axis=1, tiled=True).astype(jnp.float32)
    scaled = (portion_float * mixer_gain).astype(jnp.bfloat16)
    query_raw = jnp.dot(scaled, w_query, preferred_element_type=jnp.float32)
    key_raw = jnp.dot(scaled, key_cols, preferred_element_type=jnp.float32)
    value_raw = jnp.dot(scaled, value_cols, preferred_element_type=jnp.float32)
    squares = jnp.sum(portion_float * portion_float, axis=1)
    inv_rms = lax.rsqrt(squares / D + EPSILON)[:, None]
    queries = head_norm(query_raw.reshape(rows_local, heads_local, HEAD), query_gain).astype(
        jnp.bfloat16
    )
    keys_own = head_norm(key_raw, key_gain).astype(jnp.bfloat16)
    values_own = (value_raw * inv_rms).astype(jnp.bfloat16)
    keys_prev, values_prev = from_behind(
        (keys_own[rows_local - WINDOW :], values_own[rows_local - WINDOW :]), "ep", 1
    )
    first_row = lax.axis_index("ep") * rows_local
    attended = band_attend(
        queries, keys_own, values_own, keys_prev, values_prev, sink_logit, first_row
    )
    head_partial = jnp.dot(attended, w_output, preferred_element_type=jnp.float32)
    mixer_output = lax.psum_scatter(
        head_partial.astype(jnp.bfloat16), "tp", scatter_dimension=1, tiled=True
    )
    tokens_local = expert_input.shape[0]
    expert_float = expert_input.astype(jnp.float32)
    normed = (
        expert_float
        * lax.rsqrt(jnp.mean(expert_float * expert_float, axis=-1, keepdims=True) + EPSILON)
        * expert_gain
    ).astype(jnp.bfloat16)
    capacity = 2 * tokens_local * TOPK // ep_count
    flat_ids = route_ids.reshape(-1)
    onehot = (flat_ids[:, None] == jnp.arange(ep_count, dtype=jnp.int32)[None, :]).astype(jnp.int32)
    earlier = jnp.cumsum(onehot, axis=0) - onehot
    slot_index = jnp.sum(earlier * onehot, axis=-1)
    slot_column = flat_ids * capacity + slot_index
    token_ids = jnp.arange(tokens_local * TOPK, dtype=jnp.int32) // TOPK
    slot_table = (
        jnp.full((ep_count * capacity,), tokens_local, jnp.int32).at[slot_column].set(token_ids)
    )
    col_width = expert_down.shape[2]
    arrived_rows = ep_count * capacity
    own_columns = lax.dynamic_slice_in_dim(normed, lax.axis_index("tp") * col_width, col_width, 1)
    padded = jnp.concatenate([own_columns, jnp.zeros((1, col_width), jnp.bfloat16)], axis=0)
    outgoing = padded[slot_table].reshape(ep_count, capacity, col_width)
    arrived = lax.all_to_all(outgoing, "ep", split_axis=0, concat_axis=0, tiled=True).reshape(
        arrived_rows, col_width
    )
    portion = lax.all_gather(arrived, "tp", axis=1, tiled=True)
    gate_part = expert_gate[0]
    up_part = expert_up[0]
    gate_pre = jnp.dot(portion, gate_part, preferred_element_type=jnp.float32)
    up_pre = jnp.dot(portion, up_part, preferred_element_type=jnp.float32)
    routed_hidden = (jax.nn.silu(gate_pre) * up_pre).astype(jnp.bfloat16)
    shared_hidden = (
        jax.nn.silu(jnp.dot(normed, shared_gate, preferred_element_type=jnp.float32))
        * jnp.dot(normed, shared_up, preferred_element_type=jnp.float32)
    ).astype(jnp.bfloat16)
    routed_part = expert_down[0]
    routed_sum = jnp.dot(
        lax.all_gather(routed_hidden, "tp", axis=1, tiled=True),
        routed_part,
        preferred_element_type=jnp.float32,
    )
    shared_sum = jnp.dot(
        lax.all_gather(shared_hidden, "tp", axis=1, tiled=True),
        shared_down,
        preferred_element_type=jnp.float32,
    )
    expert_rows = routed_sum.astype(jnp.bfloat16).reshape(ep_count, capacity, col_width)
    returned = lax.all_to_all(expert_rows, "ep", split_axis=0, concat_axis=0, tiled=True).reshape(
        arrived_rows, col_width
    )
    picked = returned[slot_column].reshape(tokens_local, TOPK, col_width).astype(jnp.float32)
    expert_output = (shared_sum + jnp.sum(picked * route_weight[:, :, None], axis=1)).astype(
        jnp.bfloat16
    )
    return (mixer_output, expert_output)


def solution(mesh):
    in_specs = (
        P("ep", "tp"),
        P(),
        P(None, "tp"),
        P(),
        P(),
        P(),
        P(),
        P("tp"),
        P("tp", None),
        P("ep", None),
        P(),
        P("ep", None),
        P("ep", None),
        P("ep", None, "tp"),
        P("ep", None, "tp"),
        P("ep", None, "tp"),
        P(None, "tp"),
        P(None, "tp"),
        P(None, "tp"),
    )
    out_specs = (P("ep", "tp"), P("ep", "tp"))
    return jax.shard_map(shards, mesh=mesh, in_specs=in_specs, out_specs=out_specs, check_vma=False)
```

profile of v0, /device:TPU:0, one launch (start us, length us, event | category | flops | bytes accessed | tf_op | source)
XLA Modules:
  0.0 198.8 jit_solution(15007778299557219078)
XLA Ops:
  7.2 0.8 broadcast_multiply_fusion
  8.1 0.8 copy.36
  9.1 1.2 fusion.29
  10.5 1.1 reduce-window.6
  12.1 2.4 %scatter_custom_fusion = s32[1024]{0:T(1024)S(1)} fusion(s32[512]{0:T(512)S(1)} %bitcast.93, s32[512]{0:T(512)S(1)} %add_select_fusion, s32[]{:T(128)} %constant.39.clone.1), kind=kCustom, calls=%fused_computation.89 | custom fusion | bytes 4100 | tf_op jit(solution)/shard_map/scatter | solution.py:139
  14.5 1.2 fusion.31
  15.8 0.7 copy-done.2
  16.6 4.0 %gather_fusion = bf16[1024,512]{1,0:T(8,128)(2,1)S(1)} fusion(bf16[129,512]{1,0:T(8,128)(2,1)S(1)} %concatenate.19, s32[1024]{0:T(1024)S(1)} %fusion.53), kind=kCustom, calls=%fused_computation | custom fusion | bytes 2101248 | tf_op jit(solution)/shard_map/gather | solution.py:145
  20.5 32.9 %all_to_all.10 = bf16[8,128,512]{2,1,0:T(8,128)(2,1)} all-to-all(bf16[8,128,512]{2,1,0:T(8,128)(2,1)S(1)} %bitcast.89), channel_id=1, replica_groups=mesh['ep'=8,'tp'=4] {'ep'}, dimensions={0} | all-to-all | bytes 2097152 | tf_op jit(solution)/shard_map/all_to_all | solution.py:146
  54.3 32.9 %all-gather.6.cloned.1.call-done = bf16[1024,2048]{1,0:T(8,128)(2,1)} async-done(((bf16[1024,512]{1,0:T(8,128)(2,1)}), bf16[1024,2048]{1,0:T(8,128)(2,1)}) %all-gather.6.cloned.1.call-update) | async-done | bytes 4194320 | tf_op jit(solution)/shard_map/all_gather | solution.py:149
  87.2 4.7 %fusion.4 = f32[1024,512]{1,0:T(8,128)S(1)} fusion(bf16[1024,2048]{1,0:T(8,128)(2,1)} %all-gather.6.cloned.1.call-done, bf16[1,2048,512]{2,1,0:T(8,128)(2,1)S(1)} %copy-done), kind=kOutput, calls=%fused_computation.10 | convolution fusion | flops 2147483648 | bytes 8388608 | tf_op jit(solution)/shard_map/dot_general | solution.py:153
  91.8 3.7 %multiply_convert_fusion = bf16[1024,512]{1,0:T(8,128)(2,1)} fusion(f32[1024,512]{1,0:T(8,128)S(1)} %fusion.4, bf16[1024,2048]{1,0:T(8,128)(2,1)S(1)} %copy-done.9, bf16[1,2048,512]{2,1,0:T(8,128)(2,1)S(1)} %copy-done.10), kind=kOutput, calls=%fused_computation.15 | convolution fusion | flops 2150629376 | bytes 9437184 | tf_op jit(solution)/shard_map/dot_general | solution.py:152
  96.0 15.4 %all-gather.4.cloned.1.call-done = bf16[512,2048]{1,0:T(8,128)(2,1)} async-done(((bf16[512,512]{1,0:T(8,128)(2,1)}), bf16[512,2048]{1,0:T(8,128)(2,1)}) %all-gather.4.cloned.1.call-update) | async-done | bytes 2097168 | tf_op jit(solution)/shard_map/all_gather | solution.py:101
  111.3 2.2 %fusion.1 = f32[512]{0:T(512)S(1)} fusion(bf16[512,2048]{1,0:T(8,128)(2,1)} %all-gather.4.cloned.1.call-done), kind=kLoop, calls=%fused_computation.6 | loop fusion | flops 3145216 | bytes 2099200 | tf_op jit(solution)/shard_map/reduce_sum | solution.py:106
  113.6 1.0 fusion.26
  115.2 4.0 %collective-permute-start = (bf16[128,64]{0,1:T(8,128)(2,1)}, bf16[128,64]{0,1:T(8,128)(2,1)}, u32[]{:S(2)}, u32[]{:S(2)}) collective-permute-start(bf16[128,64]{0,1:T(8,128)(2,1)} %slice.28), channel_id=1, source_target_pairs={{0,4},{4,8},{8,12},{12,16},{16,20},{20,24},{24,28},{1,5},{5,9},{9,... | collective-permute-start | bytes 49160 | tf_op jit(solution)/shard_map/ppermute | solution.py:19
  119.1 1.0 multiply_reduce_fusion.1
  120.4 0.8 bitcast_reduce_fusion
  121.8 3.4 %collective-permute-start.1 = (bf16[128,64]{0,1:T(8,128)(2,1)}, bf16[128,64]{0,1:T(8,128)(2,1)}, u32[]{:S(2)}, u32[]{:S(2)}) collective-permute-start(bf16[128,64]{0,1:T(8,128)(2,1)} %slice.29), channel_id=1, source_target_pairs={{0,4},{4,8},{8,12},{12,16},{16,20},{20,24},{24,28},{1,5},{5,9},{9,... | collective-permute-start | bytes 49160 | tf_op jit(solution)/shard_map/ppermute | solution.py:19
  125.3 0.7 copy_bitcast_fusion.3
  126.9 1.2 fusion.63
  129.8 2.1 %convolution_convert_fusion = bf16[512,2048]{1,0:T(8,128)(2,1)} fusion(bf16[256,2048]{1,0:T(8,128)(2,1)S(1)} %copy-done.3, bf16[32,8,4,128]{3,2,1,0:T(4,128)(2,1)S(1)} %bitcast.92), kind=kOutput, calls=%fused_computation.7 | convolution fusion | flops 537919488 | bytes 3407872 | tf_op jit(solution)/shard_map/dot_general | solution.py:120
  131.9 15.5 %all-gather.8.cloned.1.call-done = bf16[1024,2048]{1,0:T(8,128)(2,1)} async-done(((bf16[1024,512]{1,0:T(8,128)(2,1)}), bf16[1024,2048]{1,0:T(8,128)(2,1)}) %all-gather.8.cloned.1.call-update) | async-done | bytes 4194320 | tf_op jit(solution)/shard_map/all_gather | solution.py:161
  147.4 6.2 %fusion.17 = bf16[1024,512]{1,0:T(8,128)(2,1)} fusion(bf16[1024,2048]{1,0:T(8,128)(2,1)} %all-gather.8.cloned.1.call-done, bf16[1,2048,512]{2,1,0:T(8,128)(2,1)} %param.34), kind=kOutput, calls=%fused_computation.22 | convolution fusion | flops 2148007936 | bytes 7340032 | tf_op jit(solution)/shard_map/dot_general | solution.py:160
  153.6 5.6 %all-to-all-start.1 = ((bf16[8,128,512]{2,1,0:T(8,128)(2,1)}), bf16[8,128,512]{2,1,0:T(8,128)(2,1)S(1)}, u32[]{:S(2)}, u32[]{:S(2)}) async-start(bf16[8,128,512]{2,1,0:T(8,128)(2,1)} %bitcast.91), calls=%async_computation.2 | async-start | bytes 2097152 | tf_op jit(solution)/shard_map/all_to_all | solution.py:171
  159.3 1.7 fusion.64
  161.1 1.7 fusion.25
  162.8 5.8 %all_gather.13 = bf16[128,1024]{1,0:T(8,128)(2,1)S(1)} all-gather(bf16[128,256]{1,0:T(8,128)(2,1)S(1)} %fusion.25), channel_id=1, replica_groups=mesh['ep'=8,'tp'=4] {'tp'}, dimensions={1}, use_global_device_ids=true | all-gather | bytes 327680 | tf_op jit(solution)/shard_map/all_gather | solution.py:166
  168.6 16.8 %all-to-all-done.1 = bf16[8,128,512]{2,1,0:T(8,128)(2,1)S(1)} async-done(((bf16[8,128,512]{2,1,0:T(8,128)(2,1)}), bf16[8,128,512]{2,1,0:T(8,128)(2,1)S(1)}, u32[]{:S(2)}, u32[]{:S(2)}) %all-to-all-start.1) | async-done | bytes 1048608 | tf_op jit(solution)/shard_map/all_to_all | solution.py:171
  185.4 2.6 %gather_fusion.1 = bf16[512,512]{1,0:T(8,128)(2,1)} fusion(bf16[1024,512]{1,0:T(8,128)(2,1)S(1)} %bitcast.88, s32[1024]{0:T(1024)S(1)} %pad_clamp_fusion), kind=kCustom, calls=%fused_computation.1 | custom fusion | bytes 1050624 | tf_op jit(solution)/shard_map/gather | solution.py:174
  188.0 1.4 reshape.216
  190.1 2.2 %fusion.21 = bf16[128,512]{1,0:T(8,128)(2,1)} fusion(f32[128,512]{1,0:T(8,128)S(1)} %multiply_reduce_fusion, bf16[128,1024]{1,0:T(8,128)(2,1)S(1)} %all_gather.13, bf16[1024,512]{1,0:T(8,128)(2,1)} %param.37), kind=kOutput, calls=%fused_computation.28 | convolution fusion | flops 134348800 | bytes 1703936 | tf_op jit(solution)/shard_map/dot_general | solution.py:165
  (74 shorter events, 7.1 us)
Async XLA Ops:
  7.2 80.0 %copy-start = (bf16[1,2048,512]{2,1,0:T(8,128)(2,1)S(1)}, bf16[1,2048,512]{2,1,0:T(8,128)(2,1)}, u32[]{:S(2)}) copy-start(bf16[1,2048,512]{2,1,0:T(8,128)(2,1)} %param.33) | copy-start | bytes 6291460
  7.2 80.0 %all-gather.6.cloned.1.call-start = ((), (), s32[]{:S(2)}) async-start(), calls=%async_computation.5 | async-start | bytes 5242880 | tf_op jit(solution)/shard_map/all_gather | solution.py:149
  15.8 0.8 copy-start.2
  53.5 57.8 %all-gather.4.cloned.1.call-start = ((), (), s32[]{:S(2)}) async-start(), calls=%async_computation.3 | async-start | bytes 2621440 | tf_op jit(solution)/shard_map/all_gather | solution.py:101
  54.3 93.1 %all-gather.8.cloned.1.call-start = ((), (), s32[]{:S(2)}) async-start(), calls=%async_computation.6 | async-start | bytes 5242880 | tf_op jit(solution)/shard_map/all_gather | solution.py:161
  87.2 4.7 %copy-start.9 = (bf16[1024,2048]{1,0:T(8,128)(2,1)S(1)}, bf16[1024,2048]{1,0:T(8,128)(2,1)}, u32[]{:S(2)}) copy-start(bf16[1024,2048]{1,0:T(8,128)(2,1)} %all-gather.6.cloned.1.call-done) | copy-start | bytes 12582916
  87.2 4.7 %copy-start.10 = (bf16[1,2048,512]{2,1,0:T(8,128)(2,1)S(1)}, bf16[1,2048,512]{2,1,0:T(8,128)(2,1)}, u32[]{:S(2)}) copy-start(bf16[1,2048,512]{2,1,0:T(8,128)(2,1)} %param.32) | copy-start | bytes 6291460
  95.5 18.1 %copy-start.5 = (f32[2048]{0:T(1024)S(1)}, f32[2048]{0:T(1024)}, u32[]{:S(2)}) copy-start(f32[2048]{0:T(1024)} %param.20) | copy-start | bytes 24580
  95.5 18.1 %copy-start.12 = (bf16[2048,128]{1,0:T(8,128)(2,1)S(1)}, bf16[2048,128]{1,0:T(8,128)(2,1)}, u32[]{:S(2)}) copy-start(bf16[2048,128]{1,0:T(8,128)(2,1)} %param.23) | copy-start | bytes 1572868
  95.5 96.8 %reduce-scatter.2.cloned.1.call-start = ((), (), s32[]{:S(2)}) async-start(), calls=%async_computation.4 | async-start | bytes 2621440 | tf_op jit(solution)/shard_map/reduce_scatter | solution.py:121
  111.3 2.3 %copy-start.1 = (bf16[512,2048]{1,0:T(8,128)(2,1)S(1)}, bf16[512,2048]{1,0:T(8,128)(2,1)}, u32[]{:S(2)}) copy-start(bf16[512,2048]{1,0:T(8,128)(2,1)} %all-gather.4.cloned.1.call-done) | copy-start | bytes 6291460
  111.3 7.8 %copy-start.4 = (bf16[2048,128]{1,0:T(8,128)(2,1)S(1)}, bf16[2048,128]{1,0:T(8,128)(2,1)}, u32[]{:S(2)}) copy-start(bf16[2048,128]{1,0:T(8,128)(2,1)} %param.22) | copy-start | bytes 1572868
  114.5 5.6 %copy-start.6 = (f32[64]{0:T(128)S(1)}, f32[64]{0:T(128)}, u32[]{:S(2)}) copy-start(f32[64]{0:T(128)} %param.25) | copy-start | bytes 772
  114.5 5.8 %copy-start.11 = (bf16[2048,256]{1,0:T(8,128)(2,1)S(1)}, bf16[2048,256]{1,0:T(8,128)(2,1)}, u32[]{:S(2)}) copy-start(bf16[2048,256]{1,0:T(8,128)(2,1)} %param.21) | copy-start | bytes 3145732
  115.2 10.2 %collective-permute-start = (bf16[128,64]{0,1:T(8,128)(2,1)}, bf16[128,64]{0,1:T(8,128)(2,1)}, u32[]{:S(2)}, u32[]{:S(2)}) collective-permute-start(bf16[128,64]{0,1:T(8,128)(2,1)} %slice.28), channel_id=1, source_target_pairs={{0,4},{4,8},{8,12},{12,16},{16,20},{20,24},{24,28},{1,5},{5,9},{9,... | collective-permute-start | bytes 49160 | tf_op jit(solution)/shard_map/ppermute | solution.py:19
  121.8 4.4 %collective-permute-start.1 = (bf16[128,64]{0,1:T(8,128)(2,1)}, bf16[128,64]{0,1:T(8,128)(2,1)}, u32[]{:S(2)}, u32[]{:S(2)}) collective-permute-start(bf16[128,64]{0,1:T(8,128)(2,1)} %slice.29), channel_id=1, source_target_pairs={{0,4},{4,8},{8,12},{12,16},{16,20},{20,24},{24,28},{1,5},{5,9},{9,... | collective-permute-start | bytes 49160 | tf_op jit(solution)/shard_map/ppermute | solution.py:19
  125.2 3.0 %copy-start.8 = (f32[4]{0:T(128)S(1)}, f32[4]{0:T(128)}, u32[]{:S(2)}) copy-start(f32[4]{0:T(128)} %param.26) | copy-start | bytes 52
  128.6 1.2 copy-start.3
  153.6 5.7 %copy-start.7 = (f32[128,4]{0,1:T(4,128)S(1)}, f32[128,4]{0,1:T(4,128)}, u32[]{:S(2)}) copy-start(f32[128,4]{0,1:T(4,128)} %param.31) | copy-start | bytes 6148
  153.6 31.8 %all-to-all-start.1 = ((bf16[8,128,512]{2,1,0:T(8,128)(2,1)}), bf16[8,128,512]{2,1,0:T(8,128)(2,1)S(1)}, u32[]{:S(2)}, u32[]{:S(2)}) async-start(bf16[8,128,512]{2,1,0:T(8,128)(2,1)} %bitcast.91), calls=%async_computation.2 | async-start | bytes 2097152 | tf_op jit(solution)/shard_map/all_to_all | solution.py:171
Sparse Core Ops, SparseCore 0:
  53.6 33.4 all-gather.5
  88.7 22.5 all-gather.3
  112.9 34.4 all-gather.7
  150.3 31.1 reduce-scatter.1
where the time goes:
time: 199 us
  waiting for transfers between devices  81.4 us (41%)
  blocking collectives  38.7 us (19%)
  matrix products  26.6 us (13%)
  local copies, waits for them, and re-layouts  14.9 us (7%)
  between operations  14.1 us (7%)
  starting transfers between devices  13.2 us (7%)
  other arithmetic  9.96 us (5%)
    all_to_all x1, blocking collectives, shards(): lax.all_to_all(outgoing, 'ep', split_axis=0, concat_axis=0, tiled=True)  32.9 us
    all_gather x1, waiting for transfers between devices, shards(): portion = lax.all_gather(arrived, 'tp', axis=1, tiled=True)  32.9 us
    all_to_all x1, waiting for transfers between devices, shards(): lax.all_to_all(expert_rows, 'ep', split_axis=0, concat_axis=0, tiled=True)  16.8 us
    all_gather x1, waiting for transfers between devices, shards(): lax.all_gather(routed_hidden, 'tp', axis=1, tiled=True)  15.5 us
    all_gather x1, waiting for transfers between devices, shards(): lax.all_gather(mixer_input, 'tp', axis=1, tiled=True).astype(jnp.float32)  15.4 us
    ppermute x2, starting transfers between devices, from_behind(): lax.ppermute(value, axis, [(source, source + steps) for source in range(f...  7.35 us
    dot_general x1, matrix products, shards(): jnp.dot(lax.all_gather(routed_hidden, 'tp', axis=1, tiled=True), routed_p...  6.19 us
    all_gather x1, blocking collectives, shards(): lax.all_gather(shared_hidden, 'tp', axis=1, tiled=True)  5.78 us
  transfers between devices with their start and end apart: 7, of which 5 were waited for; matrix products, arithmetic and copies ran while one was open for 19% of the time, Pallas kernels for 0%

commit v1 on v0

--- a/solution.py
+++ b/solution.py
@@ -1,6 +1,10 @@
+import functools
+
 import jax
 import jax.numpy as jnp
 from jax import lax
+from jax.experimental import pallas as pl
+from jax.experimental.pallas import tpu as pltpu
 from jax.sharding import PartitionSpec as P
 
 D = 2048
@@ -70,7 +74,7 @@
     return mixed_rows.reshape(row_count, head_count * HEAD).astype(jnp.bfloat16)
 
 
-def shards(
+def shards_routed(
     mixer_input,
     mixer_gain,
     w_query,
@@ -178,6 +182,635 @@
     return (mixer_output, expert_output)
 
 
+CHUNKS = 2
+COLUMNS_X = 2
+
+
+def place_of(slot, ring):
+    half = ring // 2
+    return 0 if slot == 0 else 2 * slot - 1 if slot <= half else 2 * (ring - slot)
+
+
+def ring_position(index, ring):
+    row, side = index // COLUMNS_X, index % COLUMNS_X
+    return row + side * (ring - 1 - 2 * row)
+
+
+def ring_index(position, ring):
+    side = position // (ring // COLUMNS_X)
+    return 2 * position + side * (2 * ring - 1 - 4 * position)
+
+
+def remote(source, target, send, receive, device):
+    return pltpu.make_async_remote_copy(
+        src_ref=source,
+        dst_ref=target,
+        send_sem=send,
+        recv_sem=receive,
+        device_id=device,
+        device_id_type=pl.DeviceIdType.MESH,
+    )
+
+
+def greet(devices):
+    barrier = pltpu.get_barrier_semaphore()
+    for device in devices:
+        pl.semaphore_signal(barrier, inc=1, device_id=device, device_id_type=pl.DeviceIdType.MESH)
+    pl.semaphore_wait(barrier, len(devices))
+
+
+def limit(direction, chunk, ring):
+    return ring // 2 if direction == chunk else ring // 2 - 1
+
+
+def slot_at(direction, distance, ring):
+    return distance if direction == 0 else ring - distance
+
+
+def gather_kernel(
+    ring,
+    rows_ref,
+    gain_ref,
+    dense_ref,
+    mixer_ref,
+    gate_hbm,
+    up_hbm,
+    shared_gate_hbm,
+    shared_up_hbm,
+    mixer_out,
+    hidden_out,
+    shared_out,
+    dense_out,
+    tok,
+    gate_v,
+    up_v,
+    shared_gate_v,
+    shared_up_v,
+    load_sem,
+    ring_send,
+    ring_recv,
+    sib_send,
+    sib_recv,
+    mix_send,
+    mix_recv,
+    hid_send,
+    hid_recv,
+    sh_send,
+    sh_recv,
+    dense_send,
+    dense_recv,
+):
+    index, part = lax.axis_index("ep"), lax.axis_index("tp")
+    far, core = part // 2, part % 2
+    position = ring_position(index, ring)
+    peers = [(ring_index((position + k) % ring, ring), part) for k in range(1, ring)]
+    ahead, behind = peers[0], peers[-1]
+    sibling = (index, 2 * far + 1 - core)
+    across_part = 2 * (1 - far) + core
+    across = (index, across_part)
+    block, width = rows_ref.shape
+    piece = block // CHUNKS
+    half_width = width // 2
+    hidden_width = gate_v.shape[1]
+
+    loads = [
+        pltpu.make_async_copy(source, target, load_sem.at[i])
+        for i, (source, target) in enumerate(
+            (
+                (shared_gate_hbm, shared_gate_v),
+                (shared_up_hbm, shared_up_v),
+                (gate_hbm, gate_v),
+                (up_hbm, up_v),
+            )
+        )
+    ]
+    for load in loads:
+        load.start()
+    value = rows_ref[...].astype(jnp.float32)
+    normed = (
+        value
+        * lax.rsqrt(jnp.mean(value * value, axis=-1, keepdims=True) + EPSILON)
+        * gain_ref[...]
+    ).astype(jnp.bfloat16)
+    tok[0, pl.ds(0, block), :] = normed[:, :half_width]
+    tok[1, pl.ds(0, block), :] = normed[:, half_width:]
+
+    greet(peers + [sibling, across])
+
+    def chunk_ref(half, slot, chunk):
+        start = place_of(slot, ring) * block + chunk * piece
+        return tok.at[half, pl.ds(start, piece), :]
+
+    pending = []
+
+    def start(copy):
+        copy.start()
+        pending.append(copy)
+
+    def hop(direction, distance, chunk):
+        start(
+            remote(
+                chunk_ref(core, slot_at(direction, distance - 1, ring) % ring, chunk),
+                chunk_ref(core, slot_at(direction, distance, ring), chunk),
+                ring_send.at[direction, distance, chunk],
+                ring_recv.at[direction, distance, chunk],
+                ahead if direction == 0 else behind,
+            )
+        )
+
+    for chunk in range(CHUNKS):
+        for direction in range(2):
+            hop(direction, 1, chunk)
+    mixer_pieces = mix_send.shape[1]
+    mixer_rows = mixer_ref.shape[0] // mixer_pieces
+    mixer_cols = mixer_ref.shape[1]
+
+    def mixer_slice(owner, i):
+        return mixer_out.at[
+            pl.ds(i * mixer_rows, mixer_rows),
+            pl.ds(pl.multiple_of(owner * mixer_cols, mixer_cols), mixer_cols),
+        ]
+
+    for i in range(mixer_pieces):
+        own = mixer_ref.at[pl.ds(i * mixer_rows, mixer_rows), :]
+        start(remote(own, mixer_slice(part, i), mix_send.at[0, i], mix_recv.at[0, i], across))
+    for i in range(mixer_pieces):
+        own = mixer_ref.at[pl.ds(i * mixer_rows, mixer_rows), :]
+        start(remote(own, mixer_slice(part, i), mix_send.at[1, i], mix_recv.at[1, i], sibling))
+    keep = pltpu.make_async_copy(
+        mixer_ref,
+        mixer_out.at[:, pl.ds(pl.multiple_of(part * mixer_cols, mixer_cols), mixer_cols)],
+        load_sem.at[4],
+    )
+    keep.start()
+    for k in range(1, ring):
+        start(
+            remote(
+                dense_ref, dense_out.at[k], dense_send.at[k], dense_recv.at[k], peers[k - 1]
+            )
+        )
+    dense_out[0] = dense_ref[...]
+
+    loads[0].wait()
+    loads[1].wait()
+
+    def product(first, count, weights, columns):
+        low = tok[0, pl.ds(first, count), :]
+        high = tok[1, pl.ds(first, count), :]
+        return jnp.dot(
+            low, weights[pl.ds(0, half_width), columns], preferred_element_type=jnp.float32
+        ) + jnp.dot(
+            high,
+            weights[pl.ds(half_width, half_width), columns],
+            preferred_element_type=jnp.float32,
+        )
+
+    everything = pl.ds(0, shared_gate_v.shape[1])
+    shared_out[part] = (
+        jax.nn.silu(product(0, block, shared_gate_v, everything))
+        * product(0, block, shared_up_v, everything)
+    ).astype(jnp.bfloat16)
+    start(remote(shared_out.at[part], shared_out.at[part], sh_send.at[0], sh_recv.at[0], across))
+    start(remote(shared_out.at[part], shared_out.at[part], sh_send.at[1], sh_recv.at[1], sibling))
+    loads[2].wait()
+    loads[3].wait()
+
+    def hidden_ref(owner, slot):
+        return hidden_out.at[owner, pl.ds(place_of(slot, ring) * block, block), :]
+
+    tile = 256
+
+    def compute(slots):
+        first = min(place_of(slot, ring) for slot in slots) * block
+        count = len(slots) * block
+
+        def one(j, carry):
+            columns = pl.ds(pl.multiple_of(j * tile, tile), tile)
+            hidden_out[part, pl.ds(first, count), columns] = (
+                jax.nn.silu(product(first, count, gate_v, columns))
+                * product(first, count, up_v, columns)
+            ).astype(jnp.bfloat16)
+            return carry
+
+        lax.fori_loop(0, hidden_width // tile, one, 0)
+        for slot in slots:
+            own = hidden_ref(part, slot)
+            start(remote(own, own, hid_send.at[0, slot], hid_recv.at[0, slot], across))
+            start(remote(own, own, hid_send.at[1, slot], hid_recv.at[1, slot], sibling))
+
+    def arrive(distance):
+        for chunk in range(CHUNKS):
+            for direction in range(2):
+                if distance > limit(direction, chunk, ring):
+                    continue
+                slot = slot_at(direction, distance, ring)
+                here = chunk_ref(core, slot, chunk)
+                remote(
+                    here,
+                    here,
+                    ring_send.at[direction, distance, chunk],
+                    ring_recv.at[direction, distance, chunk],
+                    sibling,
+                ).wait_recv()
+                if distance < limit(direction, chunk, ring):
+                    hop(direction, distance + 1, chunk)
+                start(
+                    remote(
+                        here,
+                        here,
+                        sib_send.at[direction, distance, chunk],
+                        sib_recv.at[direction, distance, chunk],
+                        sibling,
+                    )
+                )
+
+    def swapped(distance):
+        for chunk in range(CHUNKS):
+            for direction in range(2):
+                if distance > limit(direction, chunk, ring):
+                    continue
+                there = chunk_ref(1 - core, slot_at(direction, distance, ring), chunk)
+                remote(
+                    there,
+                    there,
+                    sib_send.at[direction, distance, chunk],
+                    sib_recv.at[direction, distance, chunk],
+                    sibling,
+                ).wait_recv()
+
+    steps = ring // 2
+    compute([0])
+    arrive(1)
+    for distance in range(1, steps + 1):
+        if distance < steps:
+            swapped(distance)
+            compute([distance, ring - distance])
+            arrive(distance + 1)
+        else:
+            swapped(distance)
+            compute([distance])
+
+    for i in range(mixer_pieces):
+        here = mixer_slice(across_part, i)
+        remote(here, here, mix_send.at[0, i], mix_recv.at[0, i], sibling).wait_recv()
+        start(remote(here, here, mix_send.at[2, i], mix_recv.at[2, i], sibling))
+    here = shared_out.at[across_part]
+    remote(here, here, sh_send.at[0], sh_recv.at[0], sibling).wait_recv()
+    start(remote(here, here, sh_send.at[2], sh_recv.at[2], sibling))
+    order = [0]
+    for distance in range(1, steps):
+        order += [distance, ring - distance]
+    order += [steps]
+    for slot in order:
+        here = hidden_ref(across_part, slot)
+        remote(here, here, hid_send.at[0, slot], hid_recv.at[0, slot], sibling).wait_recv()
+        start(remote(here, here, hid_send.at[2, slot], hid_recv.at[2, slot], sibling))
+
+    sib_part = 2 * far + 1 - core
+    corner = 2 * (1 - far) + 1 - core
+    for path, owner in ((1, sib_part), (2, corner)):
+        for i in range(mixer_pieces):
+            here = mixer_slice(owner, i)
+            remote(here, here, mix_send.at[path, i], mix_recv.at[path, i], sibling).wait_recv()
+        here = shared_out.at[owner]
+        remote(here, here, sh_send.at[path], sh_recv.at[path], sibling).wait_recv()
+        for slot in order:
+            here = hidden_ref(owner, slot)
+            remote(
+                here, here, hid_send.at[path, slot], hid_recv.at[path, slot], sibling
+            ).wait_recv()
+    for k in range(1, ring):
+        here = dense_out.at[k]
+        remote(here, here, dense_send.at[k], dense_recv.at[k], sibling).wait_recv()
+    keep.wait()
+    for copy in pending:
+        copy.wait_send()
+
+
+def scatter_kernel(
+    ring,
+    hidden_ref,
+    weight_ref,
+    shared_ref,
+    attended_ref,
+    w_out_ref,
+    down_hbm,
+    shared_down_hbm,
+    mixer_out,
+    expert_out,
+    down_v,
+    shared_down_v,
+    mix_buf,
+    mix_got,
+    mix_sum,
+    mix_far,
+    going,
+    coming,
+    own_acc,
+    load_sem,
+    mix_send,
+    mix_recv,
+    ring_send,
+    ring_recv,
+):
+    index, part = lax.axis_index("ep"), lax.axis_index("tp")
+    far, core = part // 2, part % 2
+    position = ring_position(index, ring)
+    ahead = (ring_index((position + 1) % ring, ring), part)
+    behind = (ring_index((position + ring - 1) % ring, ring), part)
+    sibling = (index, 2 * far + 1 - core)
+    across_part = 2 * (1 - far) + core
+    across = (index, across_part)
+    parts, block, shared_width = shared_ref.shape
+    width = down_v.shape[1]
+    inner = hidden_ref.shape[2]
+    piece = block // CHUNKS
+    loads = [
+        pltpu.make_async_copy(down_hbm, down_v, load_sem.at[0]),
+        pltpu.make_async_copy(shared_down_hbm, shared_down_v, load_sem.at[1]),
+    ]
+    for load in loads:
+        load.start()
+    pending = []
+
+    def start(copy):
+        copy.start()
+        pending.append(copy)
+
+    def head_block(owner):
+        columns = pl.ds(pl.multiple_of(owner * width, width), width)
+        return jnp.dot(
+            attended_ref[...], w_out_ref[:, columns], preferred_element_type=jnp.float32
+        ).astype(jnp.bfloat16)
+
+    mix_buf[0] = head_block(2 * (1 - far) + 1 - core)
+    mix_buf[1] = head_block(2 * far + 1 - core)
+    greet([ahead, behind, sibling, across])
+    for i in range(2):
+        start(remote(mix_buf.at[i], mix_got.at[i], mix_send.at[i], mix_recv.at[i], sibling))
+    mix_buf[2] = head_block(across_part)
+    mix_buf[3] = head_block(part)
+
+    loads[0].wait()
+    steps = ring // 2
+
+    def product(slots):
+        first = min(place_of(slot, ring) for slot in slots) * block
+        count = len(slots) * block
+        total = jnp.dot(
+            hidden_ref[0, pl.ds(first, count), :],
+            down_v[pl.ds(0, inner), :],
+            preferred_element_type=jnp.float32,
+        )
+        for owner in range(1, parts):
+            total = total + jnp.dot(
+                hidden_ref[owner, pl.ds(first, count), :],
+                down_v[pl.ds(owner * inner, inner), :],
+                preferred_element_type=jnp.float32,
+            )
+        rounded = total.astype(jnp.bfloat16).astype(jnp.float32)
+        return rounded * weight_ref[pl.ds(first, count), :]
+
+    def received(direction, distance, chunk):
+        return coming.at[direction, distance, pl.ds(chunk * piece, piece), :]
+
+    def wait_for(direction, distance, chunk):
+        here = received(direction, distance, chunk)
+        remote(
+            here,
+            here,
+            ring_send.at[direction, distance, chunk],
+            ring_recv.at[direction, distance, chunk],
+            ahead,
+        ).wait_recv()
+        return here[...].astype(jnp.float32)
+
+    def push(distance, values):
+        for chunk in range(CHUNKS):
+            for direction in range(2):
+                longest = limit(direction, chunk, ring)
+                if distance > longest:
+                    continue
+                value = values[direction][chunk * piece : (chunk + 1) * piece]
+                if distance < longest:
+                    value = value + wait_for(direction, distance + 1, chunk)
+                rows = pl.ds(chunk * piece, piece)
+                going[direction, distance, rows, :] = value.astype(jnp.bfloat16)
+                start(
+                    remote(
+                        going.at[direction, distance, rows, :],
+                        received(direction, distance, chunk),
+                        ring_send.at[direction, distance, chunk],
+                        ring_recv.at[direction, distance, chunk],
+                        ahead if direction == 0 else behind,
+                    )
+                )
+
+    farthest = product([steps])
+    push(steps, (farthest, farthest))
+    for i in range(2):
+        remote(
+            mix_got.at[i], mix_got.at[i], mix_send.at[i], mix_recv.at[i], sibling
+        ).wait_recv()
+    mix_sum[...] = (
+        mix_buf[2].astype(jnp.float32) + mix_got[0].astype(jnp.float32)
+    ).astype(jnp.bfloat16)
+    start(remote(mix_sum, mix_far, mix_send.at[2], mix_recv.at[2], across))
+    for distance in range(steps - 1, 0, -1):
+        both = product([distance, ring - distance])
+        push(distance, (both[block:], both[:block]))
+    own = product([0])
+    loads[1].wait()
+    for owner in range(parts):
+        own = own + jnp.dot(
+            shared_ref[owner],
+            shared_down_v[pl.ds(owner * shared_width, shared_width), :],
+            preferred_element_type=jnp.float32,
+        )
+    own_acc[...] = own
+    for chunk in range(CHUNKS):
+        rows = pl.ds(chunk * piece, piece)
+        expert_out[rows, :] = (
+            own_acc[rows, :] + wait_for(0, 1, chunk) + wait_for(1, 1, chunk)
+        ).astype(jnp.bfloat16)
+    remote(mix_far, mix_far, mix_send.at[2], mix_recv.at[2], sibling).wait_recv()
+    mixer_out[...] = (
+        mix_buf[3].astype(jnp.float32)
+        + mix_got[1].astype(jnp.float32)
+        + mix_far[...].astype(jnp.float32)
+    ).astype(jnp.bfloat16)
+    for copy in pending:
+        copy.wait_send()
+
+
+def shards(
+    mixer_input,
+    mixer_gain,
+    w_query,
+    w_key,
+    w_value,
+    query_gain,
+    key_gain,
+    sink_logit,
+    w_output,
+    expert_input,
+    expert_gain,
+    route_ids,
+    route_weight,
+    expert_gate,
+    expert_up,
+    expert_down,
+    shared_gate,
+    shared_up,
+    shared_down,
+):
+    ring = lax.axis_size("ep")
+    parts = lax.axis_size("tp")
+    rows_local, mixer_cols = mixer_input.shape
+    tokens_local, width = expert_input.shape
+    hidden_width = expert_gate.shape[2]
+    shared_width = shared_gate.shape[1]
+    out_width = expert_down.shape[2]
+    half = ring // 2
+    vmem = pl.BlockSpec(memory_space=pltpu.VMEM)
+    hbm = pl.BlockSpec(memory_space=pl.ANY)
+    bf16, f32 = jnp.bfloat16, jnp.float32
+    dma = pltpu.SemaphoreType.DMA
+    chosen = route_ids[:, :, None] == jnp.arange(ring, dtype=jnp.int32)
+    dense = jnp.sum(jnp.where(chosen, route_weight[:, :, None], 0.0), axis=1).T
+    mixer_pieces = 4
+    mixer_full, hidden, shared_hidden, dense_all = pl.pallas_call(
+        functools.partial(gather_kernel, ring),
+        out_shape=(
+            jax.ShapeDtypeStruct((rows_local, parts * mixer_cols), bf16),
+            jax.ShapeDtypeStruct((parts, ring * tokens_local, hidden_width), bf16),
+            jax.ShapeDtypeStruct((parts, tokens_local, shared_width), bf16),
+            jax.ShapeDtypeStruct((ring, ring, tokens_local), f32),
+        ),
+        in_specs=[vmem] * 4 + [hbm] * 4,
+        out_specs=(vmem,) * 4,
+        scratch_shapes=[
+            pltpu.VMEM((2, ring * tokens_local, width // 2), bf16),
+            pltpu.VMEM((width, hidden_width), bf16),
+            pltpu.VMEM((width, hidden_width), bf16),
+            pltpu.VMEM((width, shared_width), bf16),
+            pltpu.VMEM((width, shared_width), bf16),
+            dma((5,)),
+            dma((2, half + 1, CHUNKS)),
+            dma((2, half + 1, CHUNKS)),
+            dma((2, half + 1, CHUNKS)),
+            dma((2, half + 1, CHUNKS)),
+            dma((3, mixer_pieces)),
+            dma((3, mixer_pieces)),
+            dma((3, ring)),
+            dma((3, ring)),
+            dma((3,)),
+            dma((3,)),
+            dma((ring,)),
+            dma((ring,)),
+        ],
+        compiler_params=pltpu.CompilerParams(
+            collective_id=0, has_side_effects=True, vmem_limit_bytes=48 * 1024 * 1024
+        ),
+        name="gather",
+    )(
+        expert_input,
+        expert_gain[None, :],
+        dense,
+        mixer_input,
+        expert_gate[0],
+        expert_up[0],
+        shared_gate,
+        shared_up,
+    )
+
+    heads_local = w_query.shape[1] // HEAD
+    kv_index = lax.axis_index("tp") // (parts // KV_HEADS)
+    key_cols = lax.dynamic_slice_in_dim(w_key, kv_index * HEAD, HEAD, 1)
+    value_cols = lax.dynamic_slice_in_dim(w_value, kv_index * HEAD, HEAD, 1)
+    portion_float = mixer_full.astype(jnp.float32)
+    scaled = (portion_float * mixer_gain).astype(jnp.bfloat16)
+    query_raw = jnp.dot(scaled, w_query, preferred_element_type=jnp.float32)
+    both_raw = jnp.dot(
+        scaled,
+        jnp.concatenate([key_cols, value_cols], axis=1),
+        preferred_element_type=jnp.float32,
+    )
+    squares = jnp.sum(portion_float * portion_float, axis=1)
+    inv_rms = lax.rsqrt(squares / D + EPSILON)[:, None]
+    queries = head_norm(query_raw.reshape(rows_local, heads_local, HEAD), query_gain).astype(
+        jnp.bfloat16
+    )
+    keys_own = head_norm(both_raw[:, :HEAD], key_gain).astype(jnp.bfloat16)
+    values_own = (both_raw[:, HEAD:] * inv_rms).astype(jnp.bfloat16)
+    both_own = jnp.concatenate([keys_own, values_own], axis=1)
+    both_prev = from_behind(both_own[rows_local - WINDOW :], "ep", 1)
+    first_row = lax.axis_index("ep") * rows_local
+    attended = band_attend(
+        queries,
+        keys_own,
+        values_own,
+        both_prev[:, :HEAD],
+        both_prev[:, HEAD:],
+        sink_logit,
+        first_row,
+    )
+    weight_column = lax.dynamic_index_in_dim(
+        dense_all, lax.axis_index("ep"), axis=1, keepdims=False
+    )
+    slots = [0] * ring
+    for slot in range(ring):
+        slots[place_of(slot, ring)] = slot
+    weight_column = jnp.stack([weight_column[slot] for slot in slots]).reshape(-1, 1)
+    mixer_output, expert_output = pl.pallas_call(
+        functools.partial(scatter_kernel, ring),
+        out_shape=(
+            jax.ShapeDtypeStruct((rows_local, out_width), bf16),
+            jax.ShapeDtypeStruct((tokens_local, out_width), bf16),
+        ),
+        in_specs=[vmem] * 5 + [hbm] * 2,
+        out_specs=(vmem,) * 2,
+        scratch_shapes=[
+            pltpu.VMEM(expert_down.shape[1:], bf16),
+            pltpu.VMEM(shared_down.shape, bf16),
+            pltpu.VMEM((4, rows_local, out_width), bf16),
+            pltpu.VMEM((2, rows_local, out_width), bf16),
+            pltpu.VMEM((rows_local, out_width), bf16),
+            pltpu.VMEM((rows_local, out_width), bf16),
+            pltpu.VMEM((2, half + 1, tokens_local, out_width), bf16),
+            pltpu.VMEM((2, half + 1, tokens_local, out_width), bf16),
+            pltpu.VMEM((tokens_local, out_width), f32),
+            dma((2,)),
+            dma((3,)),
+            dma((3,)),
+            dma((2, half + 1, CHUNKS)),
+            dma((2, half + 1, CHUNKS)),
+        ],
+        compiler_params=pltpu.CompilerParams(
+            collective_id=1, has_side_effects=True, vmem_limit_bytes=48 * 1024 * 1024
+        ),
+        name="scatter",
+    )(
+        hidden,
+        weight_column,
+        shared_hidden,
+        attended,
+        w_output,
+        expert_down[0],
+        shared_down,
+    )
+    return (mixer_output, expert_output)
+
+
+def plan(*arrays):
+    route_ids = arrays[11]
+    capacity = 2 * route_ids.size // lax.axis_size("ep")
+    whole_blocks = capacity >= route_ids.shape[0]
+    if whole_blocks and lax.axis_size("tp") == 4:
+        return shards(*arrays)
+    return shards_routed(*arrays)
+
+
 def solution(mesh):
     in_specs = (
         P("ep", "tp"),
@@ -201,4 +834,4 @@
         P(None, "tp"),
     )
     out_specs = (P("ep", "tp"), P("ep", "tp"))
-    return jax.shard_map(shards, mesh=mesh, in_specs=in_specs, out_specs=out_specs, check_vma=False)
+    return jax.shard_map(plan, mesh=mesh, in_specs=in_specs, out_specs=out_specs, check_vma=False)

time: 199 us -> 96.9 us (0.49)
  waiting for transfers between devices: 81.4 us -> 0.01 us
  Pallas kernels: 0 us -> 68.5 us
  blocking collectives: 38.7 us -> 0 us
  matrix products: 26.6 us -> 3.66 us
  between operations: 14.1 us -> 0.91 us
  starting transfers between devices: 13.2 us -> 3.06 us
  other arithmetic: 9.96 us -> 3.02 us
  local copies, waits for them, and re-layouts: 14.9 us -> 17.1 us
    pallas_call x0 -> x2, Pallas kernels: none -> 68.5 us  [the longest x1 48 us: shards(): pl.pallas_call(functools.partial(gather_kernel, ring), out_shape=(jax.Sha...]
    all_gather x3 -> x0, waiting for transfers between devices: 63.7 us -> none  [the longest x1 32.9 us: shards(): portion = lax.all_gather(arrived, 'tp', axis=1, tiled=True)]
    all_to_all x1 -> x0, blocking collectives: 32.9 us -> none  [shards(): lax.all_to_all(outgoing, 'ep', split_axis=0, concat_axis=0, tiled=True)]
    dot_general x9 -> x1, matrix products: 24.2 us -> 1.08 us  [shards(): jnp.dot(scaled, jnp.concatenate([key_cols, value_cols], axis=1), preferre...]
    all_to_all x1 -> x0, waiting for transfers between devices: 16.8 us -> none  [shards(): lax.all_to_all(expert_rows, 'ep', split_axis=0, concat_axis=0, tiled=True)]
    unnamed x28 -> x34, local copies, waits for them, and re-layouts: 2.21 us -> 9.54 us
    gather x2 -> x0, local copies, waits for them, and re-layouts: 6.58 us -> none  [the longest x1 3.97 us: shards(): outgoing = padded[slot_table].reshape(ep_count, capacity, col_width)]
    all_gather x1 -> x0, blocking collectives: 5.78 us -> none  [shards(): lax.all_gather(shared_hidden, 'tp', axis=1, tiled=True)]
  transfers between devices with their start and end apart: 7 -> 1, of which waited for: 5 -> 0; matrix products, arithmetic and copies ran while one was open for 19% -> 5% of each run, Pallas kernels for 0% -> 0%
where the time goes in v1:
time: 96.9 us; the launch traced here: 96.2 us
  Pallas kernels  68.5 us (71%)
  local copies, waits for them, and re-layouts  17.1 us (18%)
  matrix products  3.66 us (4%)
  starting transfers between devices  3.06 us (3%)
  other arithmetic  3.02 us (3%)
    pallas_call x1, Pallas kernels, shards(): pl.pallas_call(functools.partial(gather_kernel, ring), out_shape=(jax.Sha...  48 us
    pallas_call x1, Pallas kernels, shards(): pl.pallas_call(functools.partial(scatter_kernel, ring), out_shape=(jax.Sh...  20.5 us
    unnamed x34, local copies, waits for them, and re-layouts  9.54 us
    ppermute x1, starting transfers between devices, from_behind(): lax.ppermute(value, axis, [(source, source + steps) for source in range(f...  3.06 us
    convert_element_type x2, local copies, waits for them, and re-layouts, band_attend(): return mixed_rows.reshape(row_count, head_count * HEAD).astype(jnp.bfloat16)  2.52 us
  transfers between devices with their start and end apart: 1, of which 0 were waited for; matrix products, arithmetic and copies ran while one was open for 5% of the time, Pallas kernels for 0%

profile of v1, /device:TPU:0, one launch (start us, length us, event | category | flops | bytes accessed | tf_op | source)
XLA Modules:
  0.0 96.2 jit_solution(15838105619185707966)
XLA Ops:
  0.7 0.8 select_reduce_fusion
  1.5 1.2 %copy-done.4 = bf16[2048,256]{1,0:T(8,128)(2,1)S(1)} copy-done((bf16[2048,256]{1,0:T(8,128)(2,1)S(1)}, bf16[2048,256]{1,0:T(8,128)(2,1)}, u32[]{:S(2)}) %copy-start.4) | copy-done | bytes 1048600
  2.7 1.2 %copy-done.5 = bf16[2048,256]{1,0:T(8,128)(2,1)S(1)} copy-done((bf16[2048,256]{1,0:T(8,128)(2,1)S(1)}, bf16[2048,256]{1,0:T(8,128)(2,1)}, u32[]{:S(2)}) %copy-start.5) | copy-done | bytes 1048600
  3.9 1.0 %copy-done.6 = bf16[128,2048]{1,0:T(8,128)(2,1)S(1)} copy-done((bf16[128,2048]{1,0:T(8,128)(2,1)S(1)}, bf16[128,2048]{1,0:T(8,128)(2,1)}, u32[]{:S(2)}) %copy-start.6) | copy-done | bytes 524312
  5.0 1.0 %copy-done.7 = bf16[512,512]{1,0:T(8,128)(2,1)S(1)} copy-done((bf16[512,512]{1,0:T(8,128)(2,1)S(1)}, bf16[512,512]{1,0:T(8,128)(2,1)}, u32[]{:S(2)}) %copy-start.7) | copy-done | bytes 524312
  6.0 0.7 copy-done.8
  6.7 48.0 %gather.1 = (bf16[512,2048]{1,0:T(8,128)(2,1)S(1)}, bf16[4,1024,512]{2,1,0:T(8,128)(2,1)}, bf16[4,128,256]{2,1,0:T(8,128)(2,1)S(1)}, f32[8,8,128]{2,1,0:T(8,128)S(1)}) custom-call(bf16[128,2048]{1,0:T(8,128)(2,1)S(1)} %copy-done.6, f32[1,2048]{1,0:T(1,128)S(1)} %bitcast.67, f32[8,128]{1,0:T(8,128)S(1)} %bitcast.66, bf16[512,512]{1,0:T(8,128)(2,1)S(1)} %copy-done.7, ...), custom_call_target="tpu_custom_call" | custom-call | tf_op jit(solution)/shard_map/gather/pallas_call | solution.py:682
  54.7 0.5 fusion.1
  55.1 1.6 %constant_dynamic-slice_fusion.7 = (bf16[2048,64]{1,0:T(8,128)(2,1)S(1)}, bf16[2048,64]{1,0:T(8,128)(2,1)S(1)}) fusion(bf16[2048,128]{1,0:T(8,128)(2,1)} %param.23, s32[]{:T(128)S(6)} %select_n.24, bf16[2048,128]{1,0:T(8,128)(2,1)} %param.22), kind=kLoop, calls=%fused_computation.58 | loop fusion | bytes 1048580 | tf_op jit(solution)/shard_map/dynamic_slice | solution.py:730
  56.7 1.1 %fusion.5 = f32[512,128]{0,1:T(8,128)S(1)} fusion(bf16[512,2048]{1,0:T(8,128)(2,1)S(1)} %get-tuple-element.9, f32[2048]{0:T(1024)S(1)} %copy-done.15, bf16[2048,64]{1,0:T(8,128)(2,1)S(1)} %get-tuple-element.26, bf16[2048,64]{1,0:T(8,128)(2,1)S(1)} %get-tuple-element.27), kind=kOutput, calls=%fused_computation.9 | convolution fusion | flops 272629760 | bytes 2891776 | tf_op jit(solution)/shard_map/dot_general | solution.py:734
  57.9 0.1 fusion.16
  58.0 3.1 %collective-permute-start = (bf16[128,128]{0,1:T(8,128)(2,1)S(1)}, bf16[128,128]{0,1:T(8,128)(2,1)}, u32[]{:S(2)}, u32[]{:S(2)}) collective-permute-start(bf16[128,128]{0,1:T(8,128)(2,1)S(1)} %pad_maximum_fusion.2), channel_id=1, source_target_pairs={{0,4},{4,8},{8,12},{12,16},{16,20},{20,24},{24,28},{1,5},{5,9},{9,... | collective-permute-start | bytes 98312 | tf_op jit(solution)/shard_map/ppermute | solution.py:23
  61.1 0.6 copy_bitcast_fusion
  61.7 0.6 copy_bitcast_fusion.2
  62.3 1.6 %bitcast_reduce_fusion = (f32[512,4]{0,1:T(4,128)S(1)}, f32[512,256]{0,1:T(8,128)}) fusion(bf16[2048,256]{1,0:T(8,128)(2,1)S(1)} %copy-done, bf16[512,2048]{1,0:T(8,128)(2,1)S(1)} %get-tuple-element.9, f32[2048]{0:T(1024)S(1)} %copy-done.15), kind=kOutput, calls=%fused_computation.15 | convolution fusion | flops 540276736 | bytes 3686400 | tf_op jit(solution)/shard_map/dot_general | solution.py:733
  63.9 0.1 add_compare_fusion
  64.0 0.2 broadcast_and_fusion
  64.3 1.2 %reshape.153 = f32[4,128,4,64]{1,0,3,2:T(4,128)S(1)} reshape(f32[512,256]{0,1:T(8,128)} %get-tuple-element.23) | data formatting | bytes 1048576 | tf_op jit(solution)/shard_map/reshape | solution.py:741
  65.5 0.2 copy.48.weight_ref
  65.8 0.7 fusion.37
  66.5 0.8 copy_bitcast_fusion.3
  67.4 0.5 fusion.38
  68.0 0.3 fusion.2
  68.3 0.1 exponential_add_fusion
  68.4 0.5 fusion.7
  68.9 1.1 %copy.53 = bf16[4,128,4,64]{3,2,1,0:T(4,128)(2,1)} copy(bf16[4,128,4,64]{1,3,2,0:T(8,128)(2,1)S(1)} %fusion.7) | data formatting | bytes 524288 | tf_op jit(solution)/shard_map/convert_element_type | solution.py:74
  70.0 1.5 %reshape.156.attended_ref = bf16[512,256]{1,0:T(8,128)(2,1)S(1)} reshape(bf16[4,128,4,64]{3,2,1,0:T(4,128)(2,1)} %copy.53) | data formatting | bytes 524288 | tf_op jit(solution)/shard_map/convert_element_type | solution.py:74
  71.5 1.6 %copy-done.1 = bf16[1,2048,512]{2,1,0:T(8,128)(2,1)S(1)} copy-done((bf16[1,2048,512]{2,1,0:T(8,128)(2,1)S(1)}, bf16[1,2048,512]{2,1,0:T(8,128)(2,1)}, u32[]{:S(2)}) %copy-start.1) | copy-done | bytes 2097176
  73.0 1.2 %copy-done.3 = bf16[1024,512]{1,0:T(8,128)(2,1)S(1)} copy-done((bf16[1024,512]{1,0:T(8,128)(2,1)S(1)}, bf16[1024,512]{1,0:T(8,128)(2,1)}, u32[]{:S(2)}) %copy-start.3) | copy-done | bytes 1048600
  74.3 20.5 %scatter.1 = (bf16[512,512]{1,0:T(8,128)(2,1)S(1)}, bf16[128,512]{1,0:T(8,128)(2,1)S(1)}) custom-call(bf16[4,1024,512]{2,1,0:T(8,128)(2,1)} %get-tuple-element.6.hidden_ref, f32[1024,1]{1,0:T(8,128)S(1)} %copy.48.weight_ref, bf16[4,128,256]{2,1,0:T(8,128)(2,1)S(1)} %get-tuple-element.8.shared_ref, bf16[512,256]{1,0:T(8,128)(2,1)S(1)} %reshape.156.attended_ref, ...), custom_call_target="tpu_custom_call" | custom-call | tf_op jit(solution)/shard_map/scatter/pallas_call | solution.py:765
  94.8 0.8 copy.73
  95.6 0.7 copy.74
  (38 shorter events, 0.3 us)
Async XLA Ops:
  0.6 61.7 %copy-start = (bf16[2048,256]{1,0:T(8,128)(2,1)S(1)}, bf16[2048,256]{1,0:T(8,128)(2,1)}, u32[]{:S(2)}) copy-start(bf16[2048,256]{1,0:T(8,128)(2,1)} %param.21) | copy-start | bytes 3145732
  1.5 1.2 %copy-start.4 = (bf16[2048,256]{1,0:T(8,128)(2,1)S(1)}, bf16[2048,256]{1,0:T(8,128)(2,1)}, u32[]{:S(2)}) copy-start(bf16[2048,256]{1,0:T(8,128)(2,1)} %shared_gate_hbm.1) | copy-start | bytes 3145732
  2.7 1.2 %copy-start.5 = (bf16[2048,256]{1,0:T(8,128)(2,1)S(1)}, bf16[2048,256]{1,0:T(8,128)(2,1)}, u32[]{:S(2)}) copy-start(bf16[2048,256]{1,0:T(8,128)(2,1)} %shared_up_hbm.1) | copy-start | bytes 3145732
  3.9 1.0 %copy-start.6 = (bf16[128,2048]{1,0:T(8,128)(2,1)S(1)}, bf16[128,2048]{1,0:T(8,128)(2,1)}, u32[]{:S(2)}) copy-start(bf16[128,2048]{1,0:T(8,128)(2,1)} %rows_ref.1) | copy-start | bytes 1572868
  4.9 1.0 %copy-start.7 = (bf16[512,512]{1,0:T(8,128)(2,1)S(1)}, bf16[512,512]{1,0:T(8,128)(2,1)}, u32[]{:S(2)}) copy-start(bf16[512,512]{1,0:T(8,128)(2,1)} %mixer_ref.1) | copy-start | bytes 1572868
  6.0 0.7 copy-start.8
  54.6 2.1 %copy-start.15 = (f32[2048]{0:T(1024)S(1)}, f32[2048]{0:T(1024)}, u32[]{:S(2)}) copy-start(f32[2048]{0:T(1024)} %param.20) | copy-start | bytes 24580
  56.7 1.2 %copy-start.13 = (f32[64]{0:T(128)S(1)}, f32[64]{0:T(128)}, u32[]{:S(2)}) copy-start(f32[64]{0:T(128)} %param.25) | copy-start | bytes 772
  58.0 3.7 %copy-start.9 = (bf16[512,64]{0,1:T(8,128)(2,1)}, bf16[512,64]{0,1:T(8,128)(2,1)S(1)}, u32[]{:S(2)}) copy-start(bf16[512,64]{0,1:T(8,128)(2,1)S(1)} %get-tuple-element.10) | copy-start | bytes 196612
  58.0 7.8 %collective-permute-start = (bf16[128,128]{0,1:T(8,128)(2,1)S(1)}, bf16[128,128]{0,1:T(8,128)(2,1)}, u32[]{:S(2)}, u32[]{:S(2)}) collective-permute-start(bf16[128,128]{0,1:T(8,128)(2,1)S(1)} %pad_maximum_fusion.2), channel_id=1, source_target_pairs={{0,4},{4,8},{8,12},{12,16},{16,20},{20,24},{24,28},{1,5},{5,9},{9,... | collective-permute-start | bytes 98312 | tf_op jit(solution)/shard_map/ppermute | solution.py:23
  63.9 3.5 %copy-start.10 = (bf16[4,128,64]{1,2,0:T(8,128)(2,1)S(1)}, bf16[4,128,64]{1,2,0:T(8,128)(2,1)}, u32[]{:S(2)}) copy-start(bf16[4,128,64]{1,2,0:T(8,128)(2,1)} %copy_bitcast_fusion) | copy-start | bytes 196612
  63.9 3.5 %copy-start.14 = (f32[64]{0:T(128)S(1)}, f32[64]{0:T(128)}, u32[]{:S(2)}) copy-start(f32[64]{0:T(128)} %param.24) | copy-start | bytes 772
  65.5 2.4 %copy-start.12 = (f32[4]{0:T(128)S(1)}, f32[4]{0:T(128)}, u32[]{:S(2)}) copy-start(f32[4]{0:T(128)} %param.26) | copy-start | bytes 52
  67.4 1.0 %copy-start.11 = (bf16[4,128,64]{1,2,0:T(8,128)(2,1)S(1)}, bf16[4,128,64]{1,2,0:T(8,128)(2,1)}, u32[]{:S(2)}) copy-start(bf16[4,128,64]{1,2,0:T(8,128)(2,1)} %copy_bitcast_fusion.2) | copy-start | bytes 196612
  68.9 2.5 %copy-start.2 = (bf16[256,2048]{1,0:T(8,128)(2,1)S(1)}, bf16[256,2048]{1,0:T(8,128)(2,1)}, u32[]{:S(2)}) copy-start(bf16[256,2048]{1,0:T(8,128)(2,1)} %w_out_ref.1) | copy-start | bytes 3145732
  71.4 1.6 %copy-start.1 = (bf16[1,2048,512]{2,1,0:T(8,128)(2,1)S(1)}, bf16[1,2048,512]{2,1,0:T(8,128)(2,1)}, u32[]{:S(2)}) copy-start(bf16[1,2048,512]{2,1,0:T(8,128)(2,1)} %param.34) | copy-start | bytes 6291460
  73.0 1.2 %copy-start.3 = (bf16[1024,512]{1,0:T(8,128)(2,1)S(1)}, bf16[1024,512]{1,0:T(8,128)(2,1)}, u32[]{:S(2)}) copy-start(bf16[1024,512]{1,0:T(8,128)(2,1)} %shared_down_hbm.1) | copy-start | bytes 3145732

commit v2 on v1

--- a/solution.py
+++ b/solution.py
@@ -227,16 +227,28 @@
     return distance if direction == 0 else ring - distance
 
 
-def gather_kernel(
+def layer_kernel(
     ring,
     rows_ref,
     gain_ref,
     dense_ref,
     mixer_ref,
+    mixer_gain_ref,
+    query_gain_ref,
+    key_gain_ref,
+    sink_ref,
     gate_hbm,
     up_hbm,
     shared_gate_hbm,
     shared_up_hbm,
+    query_hbm,
+    key_hbm,
+    value_hbm,
+    w_out_hbm,
+    down_hbm,
+    shared_down_hbm,
+    mixer_result,
+    expert_out,
     mixer_out,
     hidden_out,
     shared_out,
@@ -246,7 +258,24 @@
     up_v,
     shared_gate_v,
     shared_up_v,
+    query_v,
+    key_v,
+    value_v,
+    w_out_ref,
+    down_v,
+    shared_down_v,
+    heads_ref,
+    band_ref,
+    attended_ref,
+    mix_buf,
+    mix_got,
+    mix_sum,
+    mix_far,
+    going,
+    coming,
+    own_acc,
     load_sem,
+    keep_sem,
     ring_send,
     ring_recv,
     sib_send,
@@ -259,6 +288,12 @@
     sh_recv,
     dense_send,
     dense_recv,
+    halo_send,
+    halo_recv,
+    out_send,
+    out_recv,
+    back_send,
+    back_recv,
 ):
     index, part = lax.axis_index("ep"), lax.axis_index("tp")
     far, core = part // 2, part % 2
@@ -281,6 +316,12 @@
                 (shared_up_hbm, shared_up_v),
                 (gate_hbm, gate_v),
                 (up_hbm, up_v),
+                (query_hbm, query_v),
+                (key_hbm, key_v),
+                (value_hbm, value_v),
+                (w_out_hbm, w_out_ref),
+                (down_hbm, down_v),
+                (shared_down_hbm, shared_down_v),
             )
         )
     ]
@@ -340,7 +381,7 @@
     keep = pltpu.make_async_copy(
         mixer_ref,
         mixer_out.at[:, pl.ds(pl.multiple_of(part * mixer_cols, mixer_cols), mixer_cols)],
-        load_sem.at[4],
+        keep_sem.at[0],
     )
     keep.start()
     for k in range(1, ring):
@@ -438,33 +479,35 @@
                     sibling,
                 ).wait_recv()
 
+    def forward_mixer():
+        for i in range(mixer_pieces):
+            here = mixer_slice(across_part, i)
+            remote(here, here, mix_send.at[0, i], mix_recv.at[0, i], sibling).wait_recv()
+            start(remote(here, here, mix_send.at[2, i], mix_recv.at[2, i], sibling))
+
+    def forward_hidden(slots):
+        for slot in slots:
+            here = hidden_ref(across_part, slot)
+            remote(here, here, hid_send.at[0, slot], hid_recv.at[0, slot], sibling).wait_recv()
+            start(remote(here, here, hid_send.at[2, slot], hid_recv.at[2, slot], sibling))
+
     steps = ring // 2
     compute([0])
     arrive(1)
     for distance in range(1, steps + 1):
+        swapped(distance)
         if distance < steps:
-            swapped(distance)
             compute([distance, ring - distance])
             arrive(distance + 1)
+            if distance == steps - 2:
+                forward_mixer()
         else:
-            swapped(distance)
             compute([distance])
-
-    for i in range(mixer_pieces):
-        here = mixer_slice(across_part, i)
-        remote(here, here, mix_send.at[0, i], mix_recv.at[0, i], sibling).wait_recv()
-        start(remote(here, here, mix_send.at[2, i], mix_recv.at[2, i], sibling))
-    here = shared_out.at[across_part]
-    remote(here, here, sh_send.at[0], sh_recv.at[0], sibling).wait_recv()
-    start(remote(here, here, sh_send.at[2], sh_recv.at[2], sibling))
     order = [0]
     for distance in range(1, steps):
         order += [distance, ring - distance]
     order += [steps]
-    for slot in order:
-        here = hidden_ref(across_part, slot)
-        remote(here, here, hid_send.at[0, slot], hid_recv.at[0, slot], sibling).wait_recv()
-        start(remote(here, here, hid_send.at[2, slot], hid_recv.at[2, slot], sibling))
+    forward_hidden(order[:3])
 
     sib_part = 2 * far + 1 - core
     corner = 2 * (1 - far) + 1 - core
@@ -472,6 +515,106 @@
         for i in range(mixer_pieces):
             here = mixer_slice(owner, i)
             remote(here, here, mix_send.at[path, i], mix_recv.at[path, i], sibling).wait_recv()
+    keep.wait()
+    for load in loads[4:8]:
+        load.wait()
+    rows_local = mixer_ref.shape[0]
+    query_sum = key_sum = value_sum = squares = 0.0
+    for owner in range(mixer_out.shape[1] // mixer_cols):
+        columns = pl.ds(owner * mixer_cols, mixer_cols)
+        value = mixer_out[:, columns].astype(jnp.float32)
+        squares = squares + jnp.sum(value * value, axis=1, keepdims=True)
+        scaled = (value * mixer_gain_ref[:, columns]).astype(jnp.bfloat16)
+        query_sum = query_sum + jnp.dot(
+            scaled, query_v[columns, :], preferred_element_type=jnp.float32
+        )
+        key_sum = key_sum + jnp.dot(
+            scaled, key_v[columns, :], preferred_element_type=jnp.float32
+        )
+        value_sum = value_sum + jnp.dot(
+            scaled, value_v[columns, :], preferred_element_type=jnp.float32
+        )
+    second = part // (lax.axis_size("tp") // KV_HEADS)
+    key_raw = jnp.where(second == 0, key_sum[:, :HEAD], key_sum[:, HEAD:])
+    value_raw = jnp.where(second == 0, value_sum[:, :HEAD], value_sum[:, HEAD:])
+    band_ref[pl.ds(WINDOW, rows_local), :] = jnp.concatenate(
+        [
+            head_norm(key_raw, key_gain_ref[...]),
+            value_raw * lax.rsqrt(squares / D + EPSILON),
+        ],
+        axis=1,
+    ).astype(jnp.bfloat16)
+    heads_local = heads_ref.shape[0]
+    for head in range(heads_local):
+        one_head = query_sum[:, head * HEAD : (head + 1) * HEAD]
+        heads_ref[head] = head_norm(one_head, query_gain_ref[...]).astype(jnp.bfloat16)
+    start(
+        remote(
+            band_ref.at[pl.ds(rows_local, WINDOW), :],
+            band_ref.at[pl.ds(0, WINDOW), :],
+            halo_send.at[0],
+            halo_recv.at[0],
+            ((index + 1) % ring, part),
+        )
+    )
+    forward_hidden(order[3:5])
+    halo = band_ref.at[pl.ds(0, WINDOW), :]
+    remote(halo, halo, halo_send.at[0], halo_recv.at[0], sibling).wait_recv()
+    query_rows = heads_local * WINDOW
+    row_idx = lax.broadcasted_iota(jnp.int32, (query_rows, 2 * WINDOW), 0) % WINDOW
+    key_idx = lax.broadcasted_iota(jnp.int32, (query_rows, 2 * WINDOW), 1)
+    relative = row_idx + WINDOW - key_idx
+    in_window = (relative >= 0) & (relative < WINDOW)
+
+    def attend(i, carry):
+        first = pl.multiple_of(i * WINDOW, WINDOW)
+        block_queries = heads_ref[:, pl.ds(first, WINDOW), :].reshape(query_rows, HEAD)
+        band = band_ref[pl.ds(first, 2 * WINDOW), :]
+        scores = lax.dot_general(
+            block_queries,
+            band[:, :HEAD],
+            (((1,), (1,)), ((), ())),
+            preferred_element_type=jnp.float32,
+        ) * HEAD ** (-0.5)
+        key_pos = index * rows_local + first - WINDOW + key_idx
+        masked = jnp.where(in_window & (key_pos >= 0), scores, -jnp.inf)
+        sink = sink_ref[...]
+        peak = jnp.maximum(jnp.max(masked, axis=-1, keepdims=True), sink)
+        exponent = jnp.exp(masked - peak)
+        denominator = jnp.sum(exponent, axis=-1, keepdims=True) + jnp.exp(sink - peak)
+        probability = (exponent / denominator).astype(jnp.bfloat16)
+        mixed = jnp.dot(probability, band[:, HEAD:], preferred_element_type=jnp.float32)
+        attended_ref[pl.ds(first, WINDOW), :] = jnp.concatenate(
+            [mixed[head * WINDOW : (head + 1) * WINDOW] for head in range(heads_local)], axis=1
+        ).astype(jnp.bfloat16)
+        return carry
+
+    lax.fori_loop(0, rows_local // WINDOW, attend, 0)
+
+    parts, block, shared_width = shared_out.shape
+    width = down_v.shape[1]
+    inner = hidden_out.shape[2]
+    def head_block(owner):
+        columns = pl.ds(pl.multiple_of(owner * width, width), width)
+        return jnp.dot(
+            attended_ref[...], w_out_ref[:, columns], preferred_element_type=jnp.float32
+        ).astype(jnp.bfloat16)
+
+    mix_buf[0] = head_block(2 * (1 - far) + 1 - core)
+    mix_buf[1] = head_block(2 * far + 1 - core)
+    for i in range(2):
+        start(remote(mix_buf.at[i], mix_got.at[i], out_send.at[i], out_recv.at[i], sibling))
+    mix_buf[2] = head_block(across_part)
+    mix_buf[3] = head_block(part)
+
+    forward_hidden(order[5:])
+    here = shared_out.at[across_part]
+    remote(here, here, sh_send.at[0], sh_recv.at[0], sibling).wait_recv()
+    start(remote(here, here, sh_send.at[2], sh_recv.at[2], sibling))
+    for peer in range(1, ring):
+        here = dense_out.at[peer]
+        remote(here, here, dense_send.at[peer], dense_recv.at[peer], sibling).wait_recv()
+    for path, owner in ((1, sib_part), (2, corner)):
         here = shared_out.at[owner]
         remote(here, here, sh_send.at[path], sh_recv.at[path], sibling).wait_recv()
         for slot in order:
@@ -479,97 +622,33 @@
             remote(
                 here, here, hid_send.at[path, slot], hid_recv.at[path, slot], sibling
             ).wait_recv()
-    for k in range(1, ring):
-        here = dense_out.at[k]
-        remote(here, here, dense_send.at[k], dense_recv.at[k], sibling).wait_recv()
-    keep.wait()
-    for copy in pending:
-        copy.wait_send()
-
-
-def scatter_kernel(
-    ring,
-    hidden_ref,
-    weight_ref,
-    shared_ref,
-    attended_ref,
-    w_out_ref,
-    down_hbm,
-    shared_down_hbm,
-    mixer_out,
-    expert_out,
-    down_v,
-    shared_down_v,
-    mix_buf,
-    mix_got,
-    mix_sum,
-    mix_far,
-    going,
-    coming,
-    own_acc,
-    load_sem,
-    mix_send,
-    mix_recv,
-    ring_send,
-    ring_recv,
-):
-    index, part = lax.axis_index("ep"), lax.axis_index("tp")
-    far, core = part // 2, part % 2
-    position = ring_position(index, ring)
-    ahead = (ring_index((position + 1) % ring, ring), part)
-    behind = (ring_index((position + ring - 1) % ring, ring), part)
-    sibling = (index, 2 * far + 1 - core)
-    across_part = 2 * (1 - far) + core
-    across = (index, across_part)
-    parts, block, shared_width = shared_ref.shape
-    width = down_v.shape[1]
-    inner = hidden_ref.shape[2]
-    piece = block // CHUNKS
-    loads = [
-        pltpu.make_async_copy(down_hbm, down_v, load_sem.at[0]),
-        pltpu.make_async_copy(shared_down_hbm, shared_down_v, load_sem.at[1]),
-    ]
-    for load in loads:
-        load.start()
-    pending = []
-
-    def start(copy):
-        copy.start()
-        pending.append(copy)
-
-    def head_block(owner):
-        columns = pl.ds(pl.multiple_of(owner * width, width), width)
-        return jnp.dot(
-            attended_ref[...], w_out_ref[:, columns], preferred_element_type=jnp.float32
-        ).astype(jnp.bfloat16)
-
-    mix_buf[0] = head_block(2 * (1 - far) + 1 - core)
-    mix_buf[1] = head_block(2 * far + 1 - core)
-    greet([ahead, behind, sibling, across])
-    for i in range(2):
-        start(remote(mix_buf.at[i], mix_got.at[i], mix_send.at[i], mix_recv.at[i], sibling))
-    mix_buf[2] = head_block(across_part)
-    mix_buf[3] = head_block(part)
-
-    loads[0].wait()
-    steps = ring // 2
-
-    def product(slots):
+    loads[8].wait()
+    diagonal = lax.broadcasted_iota(jnp.int32, (block, block), 0) == lax.broadcasted_iota(
+        jnp.int32, (block, block), 1
+    )
+
+    def weight_column(slot):
+        row = dense_out[slot, pl.ds(index, 1), :]
+        return jnp.sum(jnp.where(diagonal, row, 0.0), axis=1, keepdims=True)
+
+
+    def weighted(slots):
         first = min(place_of(slot, ring) for slot in slots) * block
         count = len(slots) * block
         total = jnp.dot(
-            hidden_ref[0, pl.ds(first, count), :],
+            hidden_out[0, pl.ds(first, count), :],
             down_v[pl.ds(0, inner), :],
             preferred_element_type=jnp.float32,
         )
         for owner in range(1, parts):
             total = total + jnp.dot(
-                hidden_ref[owner, pl.ds(first, count), :],
+                hidden_out[owner, pl.ds(first, count), :],
                 down_v[pl.ds(owner * inner, inner), :],
                 preferred_element_type=jnp.float32,
             )
         rounded = total.astype(jnp.bfloat16).astype(jnp.float32)
-        return rounded * weight_ref[pl.ds(first, count), :]
+        ordered = sorted(slots, key=lambda slot: place_of(slot, ring))
+        return rounded * jnp.concatenate([weight_column(slot) for slot in ordered], axis=0)
 
     def received(direction, distance, chunk):
         return coming.at[direction, distance, pl.ds(chunk * piece, piece), :]
@@ -579,8 +658,8 @@
         remote(
             here,
             here,
-            ring_send.at[direction, distance, chunk],
-            ring_recv.at[direction, distance, chunk],
+            back_send.at[direction, distance, chunk],
+            back_recv.at[direction, distance, chunk],
             ahead,
         ).wait_recv()
         return here[...].astype(jnp.float32)
@@ -600,30 +679,30 @@
                     remote(
                         going.at[direction, distance, rows, :],
                         received(direction, distance, chunk),
-                        ring_send.at[direction, distance, chunk],
-                        ring_recv.at[direction, distance, chunk],
+                        back_send.at[direction, distance, chunk],
+                        back_recv.at[direction, distance, chunk],
                         ahead if direction == 0 else behind,
                     )
                 )
 
-    farthest = product([steps])
+    farthest = weighted([steps])
     push(steps, (farthest, farthest))
     for i in range(2):
         remote(
-            mix_got.at[i], mix_got.at[i], mix_send.at[i], mix_recv.at[i], sibling
+            mix_got.at[i], mix_got.at[i], out_send.at[i], out_recv.at[i], sibling
         ).wait_recv()
     mix_sum[...] = (
         mix_buf[2].astype(jnp.float32) + mix_got[0].astype(jnp.float32)
     ).astype(jnp.bfloat16)
-    start(remote(mix_sum, mix_far, mix_send.at[2], mix_recv.at[2], across))
+    start(remote(mix_sum, mix_far, out_send.at[2], out_recv.at[2], across))
     for distance in range(steps - 1, 0, -1):
-        both = product([distance, ring - distance])
+        both = weighted([distance, ring - distance])
         push(distance, (both[block:], both[:block]))
-    own = product([0])
-    loads[1].wait()
+    own = weighted([0])
+    loads[9].wait()
     for owner in range(parts):
         own = own + jnp.dot(
-            shared_ref[owner],
+            shared_out[owner],
             shared_down_v[pl.ds(owner * shared_width, shared_width), :],
             preferred_element_type=jnp.float32,
         )
@@ -633,8 +712,8 @@
         expert_out[rows, :] = (
             own_acc[rows, :] + wait_for(0, 1, chunk) + wait_for(1, 1, chunk)
         ).astype(jnp.bfloat16)
-    remote(mix_far, mix_far, mix_send.at[2], mix_recv.at[2], sibling).wait_recv()
-    mixer_out[...] = (
+    remote(mix_far, mix_far, out_send.at[2], out_recv.at[2], sibling).wait_recv()
+    mixer_result[...] = (
         mix_buf[3].astype(jnp.float32)
         + mix_got[1].astype(jnp.float32)
         + mix_far[...].astype(jnp.float32)
@@ -679,23 +758,44 @@
     chosen = route_ids[:, :, None] == jnp.arange(ring, dtype=jnp.int32)
     dense = jnp.sum(jnp.where(chosen, route_weight[:, :, None], 0.0), axis=1).T
     mixer_pieces = 4
-    mixer_full, hidden, shared_hidden, dense_all = pl.pallas_call(
-        functools.partial(gather_kernel, ring),
+    heads_local = w_query.shape[1] // HEAD
+    vm = pltpu.VMEM
+    return pl.pallas_call(
+        functools.partial(layer_kernel, ring),
         out_shape=(
-            jax.ShapeDtypeStruct((rows_local, parts * mixer_cols), bf16),
-            jax.ShapeDtypeStruct((parts, ring * tokens_local, hidden_width), bf16),
-            jax.ShapeDtypeStruct((parts, tokens_local, shared_width), bf16),
-            jax.ShapeDtypeStruct((ring, ring, tokens_local), f32),
+            jax.ShapeDtypeStruct((rows_local, out_width), bf16),
+            jax.ShapeDtypeStruct((tokens_local, out_width), bf16),
         ),
-        in_specs=[vmem] * 4 + [hbm] * 4,
-        out_specs=(vmem,) * 4,
+        in_specs=[vmem] * 8 + [hbm] * 10,
+        out_specs=(vmem,) * 2,
         scratch_shapes=[
-            pltpu.VMEM((2, ring * tokens_local, width // 2), bf16),
-            pltpu.VMEM((width, hidden_width), bf16),
-            pltpu.VMEM((width, hidden_width), bf16),
-            pltpu.VMEM((width, shared_width), bf16),
-            pltpu.VMEM((width, shared_width), bf16),
-            dma((5,)),
+            vm((rows_local, parts * mixer_cols), bf16),
+            vm((parts, ring * tokens_local, hidden_width), bf16),
+            vm((parts, tokens_local, shared_width), bf16),
+            vm((ring, ring, tokens_local), f32),
+            vm((2, ring * tokens_local, width // 2), bf16),
+            vm((width, hidden_width), bf16),
+            vm((width, hidden_width), bf16),
+            vm((width, shared_width), bf16),
+            vm((width, shared_width), bf16),
+            vm(w_query.shape, bf16),
+            vm(w_key.shape, bf16),
+            vm(w_value.shape, bf16),
+            vm(w_output.shape, bf16),
+            vm(expert_down.shape[1:], bf16),
+            vm(shared_down.shape, bf16),
+            vm((heads_local, rows_local, HEAD), bf16),
+            vm((WINDOW + rows_local, 2 * HEAD), bf16),
+            vm((rows_local, heads_local * HEAD), bf16),
+            vm((4, rows_local, out_width), bf16),
+            vm((2, rows_local, out_width), bf16),
+            vm((rows_local, out_width), bf16),
+            vm((rows_local, out_width), bf16),
+            vm((2, half + 1, tokens_local, out_width), bf16),
+            vm((2, half + 1, tokens_local, out_width), bf16),
+            vm((tokens_local, out_width), f32),
+            dma((10,)),
+            dma((1,)),
             dma((2, half + 1, CHUNKS)),
             dma((2, half + 1, CHUNKS)),
             dma((2, half + 1, CHUNKS)),
@@ -708,98 +808,37 @@
             dma((3,)),
             dma((ring,)),
             dma((ring,)),
-        ],
-        compiler_params=pltpu.CompilerParams(
-            collective_id=0, has_side_effects=True, vmem_limit_bytes=48 * 1024 * 1024
-        ),
-        name="gather",
-    )(
-        expert_input,
-        expert_gain[None, :],
-        dense,
-        mixer_input,
-        expert_gate[0],
-        expert_up[0],
-        shared_gate,
-        shared_up,
-    )
-
-    heads_local = w_query.shape[1] // HEAD
-    kv_index = lax.axis_index("tp") // (parts // KV_HEADS)
-    key_cols = lax.dynamic_slice_in_dim(w_key, kv_index * HEAD, HEAD, 1)
-    value_cols = lax.dynamic_slice_in_dim(w_value, kv_index * HEAD, HEAD, 1)
-    portion_float = mixer_full.astype(jnp.float32)
-    scaled = (portion_float * mixer_gain).astype(jnp.bfloat16)
-    query_raw = jnp.dot(scaled, w_query, preferred_element_type=jnp.float32)
-    both_raw = jnp.dot(
-        scaled,
-        jnp.concatenate([key_cols, value_cols], axis=1),
-        preferred_element_type=jnp.float32,
-    )
-    squares = jnp.sum(portion_float * portion_float, axis=1)
-    inv_rms = lax.rsqrt(squares / D + EPSILON)[:, None]
-    queries = head_norm(query_raw.reshape(rows_local, heads_local, HEAD), query_gain).astype(
-        jnp.bfloat16
-    )
-    keys_own = head_norm(both_raw[:, :HEAD], key_gain).astype(jnp.bfloat16)
-    values_own = (both_raw[:, HEAD:] * inv_rms).astype(jnp.bfloat16)
-    both_own = jnp.concatenate([keys_own, values_own], axis=1)
-    both_prev = from_behind(both_own[rows_local - WINDOW :], "ep", 1)
-    first_row = lax.axis_index("ep") * rows_local
-    attended = band_attend(
-        queries,
-        keys_own,
-        values_own,
-        both_prev[:, :HEAD],
-        both_prev[:, HEAD:],
-        sink_logit,
-        first_row,
-    )
-    weight_column = lax.dynamic_index_in_dim(
-        dense_all, lax.axis_index("ep"), axis=1, keepdims=False
-    )
-    slots = [0] * ring
-    for slot in range(ring):
-        slots[place_of(slot, ring)] = slot
-    weight_column = jnp.stack([weight_column[slot] for slot in slots]).reshape(-1, 1)
-    mixer_output, expert_output = pl.pallas_call(
-        functools.partial(scatter_kernel, ring),
-        out_shape=(
-            jax.ShapeDtypeStruct((rows_local, out_width), bf16),
-            jax.ShapeDtypeStruct((tokens_local, out_width), bf16),
-        ),
-        in_specs=[vmem] * 5 + [hbm] * 2,
-        out_specs=(vmem,) * 2,
-        scratch_shapes=[
-            pltpu.VMEM(expert_down.shape[1:], bf16),
-            pltpu.VMEM(shared_down.shape, bf16),
-            pltpu.VMEM((4, rows_local, out_width), bf16),
-            pltpu.VMEM((2, rows_local, out_width), bf16),
-            pltpu.VMEM((rows_local, out_width), bf16),
-            pltpu.VMEM((rows_local, out_width), bf16),
-            pltpu.VMEM((2, half + 1, tokens_local, out_width), bf16),
-            pltpu.VMEM((2, half + 1, tokens_local, out_width), bf16),
-            pltpu.VMEM((tokens_local, out_width), f32),
-            dma((2,)),
+            dma((1,)),
+            dma((1,)),
             dma((3,)),
             dma((3,)),
             dma((2, half + 1, CHUNKS)),
             dma((2, half + 1, CHUNKS)),
         ],
         compiler_params=pltpu.CompilerParams(
-            collective_id=1, has_side_effects=True, vmem_limit_bytes=48 * 1024 * 1024
+            collective_id=0, has_side_effects=True, vmem_limit_bytes=62 * 1024 * 1024
         ),
-        name="scatter",
+        name="layer",
     )(
-        hidden,
-        weight_column,
-        shared_hidden,
-        attended,
+        expert_input,
+        expert_gain[None, :],
+        dense,
+        mixer_input,
+        mixer_gain[None, :],
+        query_gain[None, :],
+        key_gain[None, :],
+        jnp.repeat(sink_logit, WINDOW)[:, None],
+        expert_gate[0],
+        expert_up[0],
+        shared_gate,
+        shared_up,
+        w_query,
+        w_key,
+        w_value,
         w_output,
         expert_down[0],
         shared_down,
     )
-    return (mixer_output, expert_output)
 
 
 def plan(*arrays):

time: 96.9 us -> 77.2 us (0.80)
  local copies, waits for them, and re-layouts: 17.1 us -> 5.02 us
  matrix products: 3.66 us -> 0 us
  starting transfers between devices: 3.06 us -> 0 us
  other arithmetic: 3.02 us -> 1.3 us
  Pallas kernels: 68.5 us -> 70 us
    unnamed x34 -> x2, local copies, waits for them, and re-layouts: 9.54 us -> 3.44 us
    dot_general x4 -> x0, matrix products: 3.66 us -> none  [the longest x1 1.56 us: shards(): query_raw = jnp.dot(scaled, w_query, preferred_element_type=jnp.float32)]
    ppermute x1 -> x0, starting transfers between devices: 3.06 us -> none  [from_behind(): lax.ppermute(value, axis, [(source, source + steps) for source in range(f...]
    reshape x4 -> x0, local copies, waits for them, and re-layouts: 2.71 us -> none  [the longest x1 1.21 us: shards(): query_raw.reshape(rows_local, heads_local, HEAD)]
    convert_element_type x2 -> x0, local copies, waits for them, and re-layouts: 2.52 us -> none  [band_attend(): return mixed_rows.reshape(row_count, head_count * HEAD).astype(jnp.bfloat16)]
    dynamic_slice x1 -> x0, local copies, waits for them, and re-layouts: 1.56 us -> none  [shards(): value_cols = lax.dynamic_slice_in_dim(w_value, kv_index * HEAD, HEAD, 1)]
    pallas_call x2 -> x1, Pallas kernels: 68.5 us -> 70 us  [shards(): pl.pallas_call(functools.partial(layer_kernel, ring), out_shape=(jax.Shap...]
  transfers between devices with their start and end apart: 1 -> 0, of which waited for: 0 -> 0; matrix products, arithmetic and copies ran while one was open for 5% -> 0% of each run, Pallas kernels for 0% -> 0%
where the time goes in v2:
time: 77.2 us; the launch traced here: 76.9 us
  Pallas kernels  70 us (91%)
  local copies, waits for them, and re-layouts  5.02 us (7%)
  other arithmetic  1.3 us (2%)
    pallas_call x1, Pallas kernels, shards(): pl.pallas_call(functools.partial(layer_kernel, ring), out_shape=(jax.Shap...  70 us
    unnamed x2, local copies, waits for them, and re-layouts  3.44 us

profile of v2, /device:TPU:0, one launch (start us, length us, event | category | flops | bytes accessed | tf_op | source)
XLA Modules:
  0.0 76.9 jit_solution(11663928686492068875)
XLA Ops:
  0.6 0.7 broadcast_in_dim.36
  1.4 1.3 %select_reduce_fusion = f32[128,8]{0,1:T(8,128)} fusion(f32[128,4]{0,1:T(4,128)} %param.31, s32[128,4]{0,1:T(4,128)} %param.30), kind=kLoop, calls=%fused_computation | loop fusion | flops 11264 | bytes 8192 | tf_op jit(solution)/shard_map/reduce_sum | solution.py:759
  2.7 0.9 %copy.26.sink_ref = f32[512,1]{1,0:T(8,128)} copy(f32[512,1]{0,1:T(1,128)S(1)} %bitcast.13) | data formatting | bytes 4096 | tf_op jit(solution)/shard_map/broadcast_in_dim;reshape | solution.py:830
  3.5 70.0 %layer.1 = (bf16[512,512]{1,0:T(8,128)(2,1)}, bf16[128,512]{1,0:T(8,128)(2,1)}) custom-call(bf16[128,2048]{1,0:T(8,128)(2,1)} %rows_ref.1, f32[1,2048]{1,0:T(1,128)} %bitcast.14, f32[8,128]{1,0:T(8,128)} %bitcast.12, bf16[512,512]{1,0:T(8,128)(2,1)} %mixer_ref.1, f32[1,2048]{1,0:T(1,128)} %bitcast.15, f32[1,64]{1,0:T(1,128)} %bitcast.16, f32[1,64]{1,0:T(1,128)} %bitcast.17, ...), custom_call_target="tpu_custom_call" | custom-call | tf_op jit(solution)/shard_map/layer/pallas_call | solution.py:763
  73.5 1.9 %copy.29 = bf16[512,512]{1,0:T(8,128)(2,1)} copy(bf16[512,512]{1,0:T(8,128)(2,1)} %get-tuple-element.4) | data formatting | bytes 1048576
  75.4 1.6 %copy.30 = bf16[128,512]{1,0:T(8,128)(2,1)} copy(bf16[128,512]{1,0:T(8,128)(2,1)} %get-tuple-element.5) | data formatting | bytes 262144
